TPU v7x, 32 devices: a whole 2x2x4 slice. The times are simulated.
32 devices in a mesh: ep: 8 (over z, x), tp: 4 (over y, core).
Axes of the slice: x: 2, y: 2, z: 4, core: 2. Of those that a mesh axis runs over, the one named last changes fastest.
Arguments:
- hidden_in: bfloat16 [256, 4096], P('ep'), may hold values from -6 to 6
- norm_gain: float32 [4096], replicated, may hold values from 0.1 to 1.9
- group_ids: int32 [256], P('ep'), may hold values from 0 to 1, as said below
- inner_ids: int32 [256, 4], P('ep'), may hold values from 0 to 7, as said below
- group_prob: float32 [256], P('ep'), may hold values from 0.25 to 1
- expert_prob: float32 [256, 4], P('ep'), may hold values from 0.1 to 1
- w_gate: bfloat16 [16, 4096, 1024], P('ep', None, 'tp'), may hold values from -0.09375 to 0.09375
- w_up: bfloat16 [16, 4096, 1024], P('ep', None, 'tp'), may hold values from -0.09375 to 0.09375
- w_down: bfloat16 [16, 1024, 4096], P('ep', None, 'tp'), may hold values from -0.1875 to 0.1875
Outputs:
- moe_out: bfloat16 [256, 4096], P('ep', 'tp')
Inputs may be any that keep to these rules, and one draw needn't show every extreme that they name: `group_ids`: among the 32 tokens of one index of ep no group is named by more than 16 tokens; one group is named by exactly 16 of them, and all of these name one common expert of it. `inner_ids`: each row names 4 different experts of the token's group.
All inputs are finite; a program needn't handle non-finite values.
Results may differ from a plain program's by a relative error of at most 0.0069.
Values may be sent and summed in bfloat16 or wider, within the bound.
No kernel may reach another device: no remote copies, remote signals or barrier semaphores. Data moves between devices by JAX's collectives and lax.ppermute only.
A program may use at most 64 MiB of HBM per device.

v0:
```python
import jax
import jax.numpy as jnp
from jax import lax
from jax.sharding import PartitionSpec as P

EPG = 8
EPS = 1e-06


def expert_block(token_rows, weights, w_gate, w_up, w_down):
    gate_proj = jnp.einsum("rd,edh->erh", token_rows, w_gate, preferred_element_type=jnp.float32)
    up_proj = jnp.einsum("rd,edh->erh", token_rows, w_up, preferred_element_type=jnp.float32)
    activation = (jax.nn.silu(gate_proj) * up_proj * weights.T[:, :, None]).astype(jnp.bfloat16)
    return jnp.einsum(
        "erh,ehd->rd",
        lax.all_gather(activation, "tp", axis=2, tiled=True),
        w_down,
        preferred_element_type=jnp.float32,
    )


def on_device(
    hidden_in, norm_gain, group_ids, inner_ids, group_prob, expert_prob, w_gate, w_up, w_down
):
    widened = hidden_in.astype(jnp.float32)
    normed = (
        widened * lax.rsqrt(jnp.mean(widened * widened, axis=-1, keepdims=True) + EPS) * norm_gain
    ).astype(jnp.bfloat16)
    ep_count = lax.axis_size("ep")
    local_count = w_gate.shape[0]
    expert_count = local_count * ep_count
    tok_rows = normed.shape[0]
    expert_ids = group_ids[:, None] * EPG + inner_ids
    scaled = group_prob[:, None] * expert_prob
    matches = (expert_ids[:, :, None] == jnp.arange(expert_count)[None, None, :]).astype(
        jnp.float32
    )
    route_dense = jnp.sum(matches * scaled[:, :, None], axis=1)
    capacity = tok_rows // 2
    owners = expert_ids // local_count
    routed = jnp.any(owners[:, :, None] == jnp.arange(ep_count)[None, None, :], axis=1)
    slot_index = jnp.cumsum(routed.astype(jnp.int32), axis=0) - 1
    hit_slot = slot_index.T[:, None, :] == jnp.arange(capacity)[None, :, None]
    dispatch = (routed.T[:, None, :] & hit_slot).astype(jnp.float32)
    send_rows = jnp.einsum(
        "psr,rd->psd", dispatch.astype(jnp.bfloat16), normed, preferred_element_type=jnp.float32
    ).astype(jnp.bfloat16)
    send_weights = jnp.einsum(
        "psr,rpe->pse",
        dispatch,
        route_dense.reshape(tok_rows, ep_count, local_count),
        precision=lax.Precision.HIGHEST,
    )
    got_rows = lax.all_to_all(send_rows, "ep", split_axis=0, concat_axis=0, tiled=True)
    got_weights = lax.all_to_all(send_weights, "ep", split_axis=0, concat_axis=0, tiled=True)
    partial_value = expert_block(
        got_rows.reshape(ep_count * capacity, got_rows.shape[2]),
        got_weights.reshape(ep_count * capacity, local_count),
        w_gate,
        w_up,
        w_down,
    )
    returned = lax.all_to_all(
        partial_value.reshape(ep_count, capacity, partial_value.shape[1]),
        "ep",
        split_axis=0,
        concat_axis=0,
        tiled=True,
    )
    combined = jnp.einsum("psr,psd->rd", dispatch, returned, precision=lax.Precision.HIGHEST)
    return combined.astype(jnp.bfloat16)


def solution(mesh):
    placed = (
        P("ep", None),
        P(),
        P("ep"),
        P("ep", None),
        P("ep"),
        P("ep", None),
        P("ep", None, "tp"),
        P("ep", None, "tp"),
        P("ep", None, "tp"),
    )
    return jax.shard_map(
        on_device, mesh=mesh, in_specs=placed, out_specs=P("ep", "tp"), check_vma=False
    )
```

profile of v0, /device:TPU:0, one launch (start us, length us, event | category | flops | bytes accessed | tf_op | source)
XLA Modules:
  0.0 76.7 jit_solution(13382884557020373992)
XLA Ops:
  0.0 0.7 broadcast_multiply_fusion.1
  0.7 0.7 add_select_fusion
  1.4 0.1 copy.21
  1.4 0.1 reduce_window_sum.11
  1.5 0.1 copy.22
  1.6 0.7 broadcast_multiply_fusion
  2.3 0.8 %fusion.13 = f32[8,16,2]{1,2,0:T(2,128)} fusion(f32[32,8,2]{0,2,1:T(2,128)S(1)} %bitcast.44, s32[8,32]{1,0:T(8,128)S(1)} %copy.22, pred[8,32]{1,0:T(8,128)(4,1)S(1)} %bitcast.41), kind=kOutput, calls=%fused_computation.19 | convolution fusion | flops 106496 | bytes 4352 | tf_op jit(solution)/shard_map/psr,rpe->pse/dot_general | solution.py:48
  3.1 7.3 %all-to-all-start.1 = ((f32[8,16,2]{1,2,0:T(2,128)}), f32[8,16,2]{1,2,0:T(2,128)S(1)}, u32[]{:S(2)}, u32[]{:S(2)}) async-start(f32[8,16,2]{1,2,0:T(2,128)} %fusion.13), calls=%async_computation.1 | async-start | bytes 16384 | tf_op jit(solution)/shard_map/all_to_all | solution.py:55
  10.3 1.1 %fusion.4 = f32[32]{0:T(128)S(1)} fusion(bf16[32,4096]{1,0:T(8,128)(2,1)} %param.9), kind=kLoop, calls=%fused_computation.10 | loop fusion | flops 393184 | bytes 262272 | tf_op jit(solution)/shard_map/reduce_sum | solution.py:27
  11.5 2.4 %convolution_convert_fusion = bf16[8,16,4096]{2,1,0:T(8,128)(2,1)} fusion(bf16[32,4096]{1,0:T(8,128)(2,1)} %param.9, f32[4096]{0:T(1024)} %param.10, f32[32]{0:T(128)S(1)} %add_rsqrt_fusion, s32[8,32]{1,0:T(8,128)S(1)} %copy.22, pred[8,32]{1,0:T(8,128)(4,1)S(1)} %bitcast.42), kind=kOutput, calls=%fused_computation | convolution fusion | flops 34619392 | bytes 1328512 | tf_op jit(solution)/shard_map/psr,rd->psd/dot_general | solution.py:45
  13.9 3.0 %all-to-all-done.1 = f32[8,16,2]{1,2,0:T(2,128)S(1)} async-done(((f32[8,16,2]{1,2,0:T(2,128)}), f32[8,16,2]{1,2,0:T(2,128)S(1)}, u32[]{:S(2)}, u32[]{:S(2)}) %all-to-all-start.1) | async-done | bytes 1056 | tf_op jit(solution)/shard_map/all_to_all | solution.py:55
  16.9 3.6 %all-to-all-start = ((bf16[8,16,4096]{2,1,0:T(8,128)(2,1)}), bf16[8,16,4096]{2,1,0:T(8,128)(2,1)S(1)}, u32[]{:S(2)}, u32[]{:S(2)}) async-start(bf16[8,16,4096]{2,1,0:T(8,128)(2,1)} %convolution_convert_fusion), calls=%async_computation | async-start | bytes 2097152 | tf_op jit(solution)/shard_map/all_to_all | solution.py:54
  20.4 0.1 reshape.32
  20.5 24.8 %all-to-all-done = bf16[8,16,4096]{2,1,0:T(8,128)(2,1)S(1)} async-done(((bf16[8,16,4096]{2,1,0:T(8,128)(2,1)}), bf16[8,16,4096]{2,1,0:T(8,128)(2,1)S(1)}, u32[]{:S(2)}, u32[]{:S(2)}) %all-to-all-start) | async-done | bytes 1048608 | tf_op jit(solution)/shard_map/all_to_all | solution.py:54
  45.3 0.0 copy-start.1
  45.3 3.0 %convolution_bitcast_fusion.1 = f32[2,128,256]{2,1,0:T(8,128)S(1)} fusion(bf16[128,4096,1]{1,0,2:T(8,128)(2,1)S(1)} %bitcast.38, bf16[2,4096,256]{2,1,0:T(8,128)(2,1)} %param.15), kind=kOutput, calls=%fused_computation.2 | convolution fusion | flops 536870912 | bytes 5505024 | tf_op jit(solution)/shard_map/rd,edh->erh/dot_general | solution.py:11
  48.4 0.0 copy-start
  48.4 0.4 copy-done.1
  48.8 0.8 fusion.2
  49.5 7.3 %all_gather.3 = bf16[2,128,1024]{2,1,0:T(8,128)(2,1)S(1)} all-gather(bf16[2,128,256]{2,1,0:T(8,128)(2,1)S(1)} %fusion.2), channel_id=1, replica_groups=mesh['ep'=8,'tp'=4] {'tp'}, dimensions={2}, use_global_device_ids=true | all-gather | bytes 655360 | tf_op jit(solution)/shard_map/all_gather | solution.py:16
  56.9 0.0 copy-done
  56.9 0.7 fusion.24
  57.6 18.2 %all_to_all.15 = f32[8,16,1024]{2,1,0:T(8,128)S(1)} all-to-all(f32[8,16,1024]{2,1,0:T(8,128)S(1)} %bitcast.40), channel_id=1, replica_groups=mesh['ep'=8,'tp'=4] {'ep'}, dimensions={0} | all-to-all | bytes 1048576 | tf_op jit(solution)/shard_map/all_to_all | solution.py:63
  75.8 0.9 %fusion.3 = bf16[32,1024]{1,0:T(8,128)(2,1)} fusion(f32[8,16,1024]{2,1,0:T(8,128)S(1)} %all_to_all.15, s32[8,32]{1,0:T(8,128)S(1)} %copy.22, pred[8,32]{1,0:T(8,128)(4,1)S(1)} %bitcast.43), kind=kOutput, calls=%fused_computation.7 | convolution fusion | flops 50372608 | bytes 591104 | tf_op jit(solution)/shard_map/psr,psd->rd/dot_general | solution.py:70
  (6 shorter events, 0.0 us)
Async XLA Ops:
  3.1 13.8 %all-to-all-start.1 = ((f32[8,16,2]{1,2,0:T(2,128)}), f32[8,16,2]{1,2,0:T(2,128)S(1)}, u32[]{:S(2)}, u32[]{:S(2)}) async-start(f32[8,16,2]{1,2,0:T(2,128)} %fusion.13), calls=%async_computation.1 | async-start | bytes 16384 | tf_op jit(solution)/shard_map/all_to_all | solution.py:55
  16.9 28.5 %all-to-all-start = ((bf16[8,16,4096]{2,1,0:T(8,128)(2,1)}), bf16[8,16,4096]{2,1,0:T(8,128)(2,1)S(1)}, u32[]{:S(2)}, u32[]{:S(2)}) async-start(bf16[8,16,4096]{2,1,0:T(8,128)(2,1)} %convolution_convert_fusion), calls=%async_computation | async-start | bytes 2097152 | tf_op jit(solution)/shard_map/all_to_all | solution.py:54
  45.3 3.4 %copy-start.1 = (bf16[2,4096,256]{2,1,0:T(8,128)(2,1)S(1)}, bf16[2,4096,256]{2,1,0:T(8,128)(2,1)}, u32[]{:S(2)}) copy-start(bf16[2,4096,256]{2,1,0:T(8,128)(2,1)} %param.16) | copy-start | bytes 12582916
  48.4 8.5 %copy-start = (bf16[2,1024,1024]{2,1,0:T(8,128)(2,1)S(1)}, bf16[2,1024,1024]{2,1,0:T(8,128)(2,1)}, u32[]{:S(2)}) copy-start(bf16[2,1024,1024]{2,1,0:T(8,128)(2,1)} %param.17) | copy-start | bytes 12582916
where the time goes:
time: 77.1 us; the launch traced here: 76.7 us
  waiting for transfers between devices  27.8 us (36%)
  blocking collectives  25.5 us (33%)
  starting transfers between devices  10.8 us (14%)
  matrix products  8.68 us (11%)
  other arithmetic  3.25 us (4%)
    all_to_all x1, waiting for transfers between devices, on_device(): lax.all_to_all(send_rows, 'ep', split_axis=0, concat_axis=0, tiled=True)  24.8 us
    all_to_all x1, blocking collectives, on_device(): lax.all_to_all(partial_value.reshape(ep_count, capacity, partial_value.sh...  18.2 us
    all_gather x1, blocking collectives, expert_block(): lax.all_gather(activation, 'tp', axis=2, tiled=True)  7.33 us
    all_to_all x1, starting transfers between devices, on_device(): lax.all_to_all(send_weights, 'ep', split_axis=0, concat_axis=0, tiled=True)  7.28 us
    all_to_all x1, starting transfers between devices, on_device(): lax.all_to_all(send_rows, 'ep', split_axis=0, concat_axis=0, tiled=True)  3.56 us
    dot_general x1, matrix products, expert_block(): jnp.einsum('rd,edh->erh', token_rows, w_gate, preferred_element_type=jnp....  3.04 us
    all_to_all x1, waiting for transfers between devices, on_device(): lax.all_to_all(send_weights, 'ep', split_axis=0, concat_axis=0, tiled=True)  2.97 us
    dot_general x1, matrix products, on_device(): jnp.einsum('psr,rd->psd', dispatch.astype(jnp.bfloat16), normed, preferre...  2.44 us
  transfers between devices with their start and end apart: 2, of which 2 were waited for; matrix products, arithmetic and copies ran while one was open for 5% of the time, Pallas kernels for 0%

commit v1 on v0

--- a/solution.py
+++ b/solution.py
@@ -7,15 +7,32 @@
 EPS = 1e-06
 
 
+def product_in_turn(x, axis, dim, term):
+    size, place = (lax.axis_size(axis), lax.axis_index(axis))
+    left = [(i, (i - 1) % size) for i in range(size)]
+    rows = x.shape[dim]
+    held = x
+    total = term(held, place * rows)
+    for step in range(1, size):
+        held = lax.ppermute(held, axis, left)
+        total = total + term(held, (place + step) % size * rows)
+    return total
+
+
 def expert_block(token_rows, weights, w_gate, w_up, w_down):
     gate_proj = jnp.einsum("rd,edh->erh", token_rows, w_gate, preferred_element_type=jnp.float32)
     up_proj = jnp.einsum("rd,edh->erh", token_rows, w_up, preferred_element_type=jnp.float32)
     activation = (jax.nn.silu(gate_proj) * up_proj * weights.T[:, :, None]).astype(jnp.bfloat16)
-    return jnp.einsum(
-        "erh,ehd->rd",
-        lax.all_gather(activation, "tp", axis=2, tiled=True),
-        w_down,
-        preferred_element_type=jnp.float32,
+    return product_in_turn(
+        activation,
+        "tp",
+        2,
+        lambda part, at: jnp.einsum(
+            "erh,ehd->rd",
+            part,
+            lax.dynamic_slice_in_dim(w_down, at, part.shape[2], axis=1),
+            preferred_element_type=jnp.float32,
+        ),
     )
 
 

time: 77.1 us -> 82.3 us (1.067)
  blocking collectives: 25.5 us -> 19.7 us
  waiting for transfers between devices: 27.8 us -> 33.3 us
  starting transfers between devices: 10.8 us -> 14.6 us
  local copies, waits for them, and re-layouts: 0.62 us -> 1.68 us
    all_gather x1 -> x0, blocking collectives: 7.33 us -> none  [expert_block(): lax.all_gather(activation, 'tp', axis=2, tiled=True)]
    ppermute x0 -> x3, waiting for transfers between devices: none -> 5.54 us  [product_in_turn(): held = lax.ppermute(held, axis, left)]
    ppermute x0 -> x3, starting transfers between devices: none -> 3.8 us  [product_in_turn(): held = lax.ppermute(held, axis, left)]
    all_to_all x1, blocking collectives: 18.2 us -> 19.7 us  [on_device(): lax.all_to_all(partial_value.reshape(ep_count, capacity, partial_value.sh...]
    unnamed x4, local copies, waits for them, and re-layouts: 0.39 us -> 1.45 us
  transfers between devices with their start and end apart: 2 -> 5, of which waited for: 2 -> 5; matrix products, arithmetic and copies ran while one was open for 5% -> 6% of each run, Pallas kernels for 0% -> 0%
where the time goes in v1:
time: 82.3 us; the launch traced here: 81.9 us
  waiting for transfers between devices  33.3 us (40%)
  blocking collectives  19.7 us (24%)
  starting transfers between devices  14.6 us (18%)
  matrix products  9.2 us (11%)
  other arithmetic  3.25 us (4%)
  local copies, waits for them, and re-layouts  1.68 us (2%)
    all_to_all x1, waiting for transfers between devices, on_device(): lax.all_to_all(send_rows, 'ep', split_axis=0, concat_axis=0, tiled=True)  24.8 us
    all_to_all x1, blocking collectives, on_device(): lax.all_to_all(partial_value.reshape(ep_count, capacity, partial_value.sh...  19.7 us
    all_to_all x1, starting transfers between devices, on_device(): lax.all_to_all(send_weights, 'ep', split_axis=0, concat_axis=0, tiled=True)  7.28 us
    ppermute x3, waiting for transfers between devices, product_in_turn(): held = lax.ppermute(held, axis, left)  5.54 us
    ppermute x3, starting transfers between devices, product_in_turn(): held = lax.ppermute(held, axis, left)  3.8 us
    all_to_all x1, starting transfers between devices, on_device(): lax.all_to_all(send_rows, 'ep', split_axis=0, concat_axis=0, tiled=True)  3.56 us
    dot_general x1, matrix products, expert_block(): jnp.einsum('rd,edh->erh', token_rows, w_gate, preferred_element_type=jnp....  3.04 us
    all_to_all x1, waiting for transfers between devices, on_device(): lax.all_to_all(send_weights, 'ep', split_axis=0, concat_axis=0, tiled=True)  2.97 us
  transfers between devices with their start and end apart: 5, of which 5 were waited for; matrix products, arithmetic and copies ran while one was open for 6% of the time, Pallas kernels for 0%

profile of v1, /device:TPU:0, one launch (start us, length us, event | category | flops | bytes accessed | tf_op | source)
XLA Modules:
  0.0 81.9 jit_solution(4650236980277306266)
XLA Ops:
  0.0 0.7 broadcast_multiply_fusion.1
  0.7 0.7 add_select_fusion
  1.4 0.1 copy.21
  1.4 0.1 reduce_window_sum.11
  1.5 0.1 copy.22
  1.6 0.7 broadcast_multiply_fusion
  2.3 0.8 fusion.20
  3.1 7.3 %all-to-all-start.1 = ((f32[8,16,2]{1,2,0:T(2,128)}), f32[8,16,2]{1,2,0:T(2,128)S(1)}, u32[]{:S(2)}, u32[]{:S(2)}) async-start(f32[8,16,2]{1,2,0:T(2,128)} %fusion.20), calls=%async_computation.1 | async-start | bytes 16384 | tf_op jit(solution)/shard_map/all_to_all | solution.py:72
  10.3 1.1 %fusion.11 = f32[32]{0:T(128)S(1)} fusion(bf16[32,4096]{1,0:T(8,128)(2,1)} %param.9), kind=kLoop, calls=%fused_computation.21 | loop fusion | flops 393184 | bytes 262272 | tf_op jit(solution)/shard_map/reduce_sum | solution.py:44
  11.5 2.4 %convolution_convert_fusion = bf16[8,16,4096]{2,1,0:T(8,128)(2,1)} fusion(bf16[32,4096]{1,0:T(8,128)(2,1)} %param.9, f32[4096]{0:T(1024)} %param.10, f32[32]{0:T(128)S(1)} %add_rsqrt_fusion, s32[8,32]{1,0:T(8,128)S(1)} %copy.22, pred[8,32]{1,0:T(8,128)(4,1)S(1)} %bitcast.56), kind=kOutput, calls=%fused_computation | convolution fusion | flops 34619392 | bytes 1328512 | tf_op jit(solution)/shard_map/psr,rd->psd/dot_general | solution.py:62
  13.9 3.0 %all-to-all-done.1 = f32[8,16,2]{1,2,0:T(2,128)S(1)} async-done(((f32[8,16,2]{1,2,0:T(2,128)}), f32[8,16,2]{1,2,0:T(2,128)S(1)}, u32[]{:S(2)}, u32[]{:S(2)}) %all-to-all-start.1) | async-done | bytes 1056 | tf_op jit(solution)/shard_map/all_to_all | solution.py:72
  16.9 3.6 %all-to-all-start = ((bf16[8,16,4096]{2,1,0:T(8,128)(2,1)}), bf16[8,16,4096]{2,1,0:T(8,128)(2,1)S(1)}, u32[]{:S(2)}, u32[]{:S(2)}) async-start(bf16[8,16,4096]{2,1,0:T(8,128)(2,1)} %convolution_convert_fusion), calls=%async_computation | async-start | bytes 2097152 | tf_op jit(solution)/shard_map/all_to_all | solution.py:71
  20.5 0.1 reshape.32
  20.6 24.8 %all-to-all-done = bf16[8,16,4096]{2,1,0:T(8,128)(2,1)S(1)} async-done(((bf16[8,16,4096]{2,1,0:T(8,128)(2,1)}), bf16[8,16,4096]{2,1,0:T(8,128)(2,1)S(1)}, u32[]{:S(2)}, u32[]{:S(2)}) %all-to-all-start) | async-done | bytes 1048608 | tf_op jit(solution)/shard_map/all_to_all | solution.py:71
  45.3 0.0 copy-start.1
  45.3 3.0 %convolution_bitcast_fusion.5 = f32[2,128,256]{2,1,0:T(8,128)S(1)} fusion(bf16[128,4096,1]{1,0,2:T(8,128)(2,1)S(1)} %bitcast.52, bf16[2,4096,256]{2,1,0:T(8,128)(2,1)} %param.15), kind=kOutput, calls=%fused_computation.9 | convolution fusion | flops 536870912 | bytes 5505024 | tf_op jit(solution)/shard_map/rd,edh->erh/dot_general | solution.py:23
  48.4 0.0 copy-start
  48.4 0.4 copy-done.1
  48.8 0.8 fusion.5
  49.5 0.1 collective-permute-start
  49.6 1.1 %copy-done = bf16[2,1024,1024]{2,1,0:T(8,128)(2,1)S(1)} copy-done((bf16[2,1024,1024]{2,1,0:T(8,128)(2,1)S(1)}, bf16[2,1024,1024]{2,1,0:T(8,128)(2,1)}, u32[]{:S(2)}) %copy-start) | copy-done | bytes 4194328
  50.7 0.3 convolution_bitcast_fusion.3
  51.0 1.1 %collective-permute-done = bf16[2,128,256]{2,1,0:T(8,128)(2,1)S(1)} collective-permute-done((bf16[2,128,256]{2,1,0:T(8,128)(2,1)S(1)}, bf16[2,128,256]{2,1,0:T(8,128)(2,1)S(1)}, u32[]{:S(2)}, u32[]{:S(2)}) %collective-permute-start) | collective-permute-done | bytes 131104 | tf_op jit(solution)/shard_map/ppermute | solution.py:17
  52.1 1.9 %collective-permute-start.1 = (bf16[2,128,256]{2,1,0:T(8,128)(2,1)S(1)}, bf16[2,128,256]{2,1,0:T(8,128)(2,1)S(1)}, u32[]{:S(2)}, u32[]{:S(2)}) collective-permute-start(bf16[2,128,256]{2,1,0:T(8,128)(2,1)S(1)} %collective-permute-done), channel_id=1, source_target_pairs={{0,3},{1,0},{2,1},{3,2},{4,7},{5,4},{6,5},{7,6},{8,11},{9,8},{10,9... | collective-permute-start | bytes 393224 | tf_op jit(solution)/shard_map/ppermute | solution.py:17
  54.0 0.3 fusion
  54.3 2.2 %collective-permute-done.1 = bf16[2,128,256]{2,1,0:T(8,128)(2,1)S(1)} collective-permute-done((bf16[2,128,256]{2,1,0:T(8,128)(2,1)S(1)}, bf16[2,128,256]{2,1,0:T(8,128)(2,1)S(1)}, u32[]{:S(2)}, u32[]{:S(2)}) %collective-permute-start.1) | collective-permute-done | bytes 131104 | tf_op jit(solution)/shard_map/ppermute | solution.py:17
  56.5 1.9 %collective-permute-start.2 = (bf16[2,128,256]{2,1,0:T(8,128)(2,1)S(1)}, bf16[2,128,256]{2,1,0:T(8,128)(2,1)S(1)}, u32[]{:S(2)}, u32[]{:S(2)}) collective-permute-start(bf16[2,128,256]{2,1,0:T(8,128)(2,1)S(1)} %collective-permute-done.1), channel_id=1, source_target_pairs={{0,3},{1,0},{2,1},{3,2},{4,7},{5,4},{6,5},{7,6},{8,11},{9,8},{10,9... | collective-permute-start | bytes 393224 | tf_op jit(solution)/shard_map/ppermute | solution.py:17
  58.4 0.3 fusion.1
  58.7 2.2 %collective-permute-done.2 = bf16[2,128,256]{2,1,0:T(8,128)(2,1)S(1)} collective-permute-done((bf16[2,128,256]{2,1,0:T(8,128)(2,1)S(1)}, bf16[2,128,256]{2,1,0:T(8,128)(2,1)S(1)}, u32[]{:S(2)}, u32[]{:S(2)}) %collective-permute-start.2) | collective-permute-done | bytes 131104 | tf_op jit(solution)/shard_map/ppermute | solution.py:17
  60.9 0.3 fusion.2
  61.2 19.7 %all_to_all.15 = f32[8,16,1024]{2,1,0:T(8,128)S(1)} all-to-all(f32[8,16,1024]{2,1,0:T(8,128)S(1)} %bitcast.54), channel_id=1, replica_groups=mesh['ep'=8,'tp'=4] {'ep'}, dimensions={0} | all-to-all | bytes 1048576 | tf_op jit(solution)/shard_map/all_to_all | solution.py:80
  81.0 0.9 %fusion.6 = bf16[32,1024]{1,0:T(8,128)(2,1)} fusion(f32[8,16,1024]{2,1,0:T(8,128)S(1)} %all_to_all.15, s32[8,32]{1,0:T(8,128)S(1)} %copy.22, pred[8,32]{1,0:T(8,128)(4,1)S(1)} %bitcast.57), kind=kOutput, calls=%fused_computation.14 | convolution fusion | flops 50372608 | bytes 591104 | tf_op jit(solution)/shard_map/psr,psd->rd/dot_general | solution.py:87
  (6 shorter events, 0.0 us)
Async XLA Ops:
  3.1 13.8 %all-to-all-start.1 = ((f32[8,16,2]{1,2,0:T(2,128)}), f32[8,16,2]{1,2,0:T(2,128)S(1)}, u32[]{:S(2)}, u32[]{:S(2)}) async-start(f32[8,16,2]{1,2,0:T(2,128)} %fusion.20), calls=%async_computation.1 | async-start | bytes 16384 | tf_op jit(solution)/shard_map/all_to_all | solution.py:72
  16.9 28.5 %all-to-all-start = ((bf16[8,16,4096]{2,1,0:T(8,128)(2,1)}), bf16[8,16,4096]{2,1,0:T(8,128)(2,1)S(1)}, u32[]{:S(2)}, u32[]{:S(2)}) async-start(bf16[8,16,4096]{2,1,0:T(8,128)(2,1)} %convolution_convert_fusion), calls=%async_computation | async-start | bytes 2097152 | tf_op jit(solution)/shard_map/all_to_all | solution.py:71
  45.3 3.4 %copy-start.1 = (bf16[2,4096,256]{2,1,0:T(8,128)(2,1)S(1)}, bf16[2,4096,256]{2,1,0:T(8,128)(2,1)}, u32[]{:S(2)}) copy-start(bf16[2,4096,256]{2,1,0:T(8,128)(2,1)} %param.16) | copy-start | bytes 12582916
  48.4 2.3 %copy-start = (bf16[2,1024,1024]{2,1,0:T(8,128)(2,1)S(1)}, bf16[2,1024,1024]{2,1,0:T(8,128)(2,1)}, u32[]{:S(2)}) copy-start(bf16[2,1024,1024]{2,1,0:T(8,128)(2,1)} %param.17) | copy-start | bytes 12582916
  49.5 2.6 %collective-permute-start = (bf16[2,128,256]{2,1,0:T(8,128)(2,1)S(1)}, bf16[2,128,256]{2,1,0:T(8,128)(2,1)S(1)}, u32[]{:S(2)}, u32[]{:S(2)}) collective-permute-start(bf16[2,128,256]{2,1,0:T(8,128)(2,1)S(1)} %fusion.5), channel_id=1, source_target_pairs={{0,3},{1,0},{2,1},{3,2},{4,7},{5,4},{6,5},{7,6},{8,11},{9,8},{10,9... | collective-permute-start | bytes 393224 | tf_op jit(solution)/shard_map/ppermute | solution.py:17
  52.1 4.4 %collective-permute-start.1 = (bf16[2,128,256]{2,1,0:T(8,128)(2,1)S(1)}, bf16[2,128,256]{2,1,0:T(8,128)(2,1)S(1)}, u32[]{:S(2)}, u32[]{:S(2)}) collective-permute-start(bf16[2,128,256]{2,1,0:T(8,128)(2,1)S(1)} %collective-permute-done), channel_id=1, source_target_pairs={{0,3},{1,0},{2,1},{3,2},{4,7},{5,4},{6,5},{7,6},{8,11},{9,8},{10,9... | collective-permute-start | bytes 393224 | tf_op jit(solution)/shard_map/ppermute | solution.py:17
  56.5 4.4 %collective-permute-start.2 = (bf16[2,128,256]{2,1,0:T(8,128)(2,1)S(1)}, bf16[2,128,256]{2,1,0:T(8,128)(2,1)S(1)}, u32[]{:S(2)}, u32[]{:S(2)}) collective-permute-start(bf16[2,128,256]{2,1,0:T(8,128)(2,1)S(1)} %collective-permute-done.1), channel_id=1, source_target_pairs={{0,3},{1,0},{2,1},{3,2},{4,7},{5,4},{6,5},{7,6},{8,11},{9,8},{10,9... | collective-permute-start | bytes 393224 | tf_op jit(solution)/shard_map/ppermute | solution.py:17
